TPU v7x, 32 devices: a whole 2x2x4 slice. The times are simulated.
32 devices in a mesh: fs: 16 (over z, y, x), tp: 2 (over core).
Axes of the slice: x: 2, y: 2, z: 4, core: 2. Of those that a mesh axis runs over, the one named last changes fastest.
Arguments:
- tokens: bfloat16 [12288, 2048], P('fs'), may hold values from -6 to 6
- norm_gain: float32 [2048], replicated, may hold values from 0.1 to 1.9
- up_weight: float32 [2048, 8192], P('fs', 'tp'), may hold values from -0.125 to 0.125
- up_scale: float32 [8192], P('tp'), may hold values from 0.5 to 2
- down_weight: float32 [8192, 2048], P('tp', 'fs'), may hold values from -0.0625 to 0.0625
- down_scale: float32 [2048], P('fs'), may hold values from 0.5 to 2
Outputs:
- output: bfloat16 [12288, 2048], P('fs', 'tp')
All inputs are finite; a program needn't handle non-finite values.
Results may differ from a plain program's by a relative error of at most 0.015.
Values may be sent and summed in bfloat16 or wider, within the bound.
A program may use at most 128 MiB of HBM per device.

v0:
```python
import functools

import jax
import jax.numpy as jnp
from jax import lax
from jax.experimental import pallas as pl
from jax.experimental.pallas import tpu as pltpu
from jax.sharding import PartitionSpec as P

epsilon = 1e-06


def normalise(tokens, norm_gain):
    floats = tokens.astype(jnp.float32)
    inverse = lax.rsqrt(jnp.mean(floats * floats, axis=-1, keepdims=True) + epsilon)
    return (floats * inverse * norm_gain).astype(jnp.bfloat16)


def plain(tokens, norm_gain, up_weight, up_scale, down_weight, down_scale):
    normed = normalise(tokens, norm_gain)
    up_whole = lax.all_gather(up_weight.astype(jnp.bfloat16), "fs", axis=0, tiled=True)
    up_pre = jnp.dot(normed, up_whole, preferred_element_type=jnp.float32)
    scaled = (down_weight * down_scale).astype(jnp.bfloat16)
    down_whole = lax.all_gather(scaled, "fs", axis=1, tiled=True)
    hidden = jnp.square(jax.nn.relu(up_pre * up_scale)).astype(jnp.bfloat16)
    partial_value = jnp.dot(hidden, down_whole, preferred_element_type=jnp.float32)
    return lax.psum_scatter(
        partial_value.astype(jnp.bfloat16), "tp", scatter_dimension=1, tiled=True
    )


NX, NY = 2, 2


def kernel(nz, x_ref, s_ref, up_ref, down_ref, out_ref,
           u_buf, d_buf, t_buf, h_buf, ssend, srecv, xsend, xrecv, keep,
           send_sems, recv_sems, local_sems):
    me = lax.axis_index("fs")
    c = lax.axis_index("tp")
    x = lax.rem(me, NX)
    y = lax.rem(me // NX, NY)
    z = me // (NX * NY)
    rows = x_ref.shape[0]
    depth = up_ref.shape[0]
    wide = up_ref.shape[1] // 2
    cols = down_ref.shape[1]
    pair = NX * cols

    def fs_of(zz, yy, xx):
        return (zz * NY + yy) * NX + xx

    def wrap(v):
        return lax.rem(v + 2 * nz, nz)

    target = {
        **{k: {"fs": fs_of(wrap(z + k), y, x), "tp": c} for k in range(1, nz)},
        "y": {"fs": fs_of(z, 1 - y, x), "tp": c},
        "x": {"fs": fs_of(z, y, 1 - x), "tp": c},
        "c": {"fs": me, "tp": 1 - c},
    }

    side = lax.rem(z, 2)
    peer = {"fs": fs_of(z + 1 - 2 * side, y, x), "tp": c}

    def half_of(k):
        at = pl.multiple_of(lax.rem(z + k, 2) * wide, wide)
        return up_ref.at[:, pl.ds(at, wide)], down_ref.at[pl.ds(at, wide), :]

    own_up = u_buf.at[pl.ds(pl.multiple_of(me * depth, depth), depth), :]
    own_down = d_buf.at[me // NX, :, pl.ds(pl.multiple_of(x * cols, cols), cols)]
    local = [
        pltpu.make_async_copy(half_of(0)[0], own_up, local_sems.at[0]),
        pltpu.make_async_copy(half_of(0)[1], own_down, local_sems.at[1]),
    ]
    for copy in local:
        copy.start()

    barrier = pltpu.get_barrier_semaphore()
    for where in target.values():
        pl.semaphore_signal(barrier, inc=1, device_id=where, device_id_type=pl.DeviceIdType.MESH)
    pl.semaphore_wait(barrier, len(target))

    slots, started = {}, []

    def copy_of(key, src, dst, way):
        n = slots.setdefault(key, len(slots))
        return pltpu.make_async_remote_copy(
            src_ref=src, dst_ref=dst, send_sem=send_sems.at[n], recv_sem=recv_sems.at[n],
            device_id=peer if way == "peer" else target[way], device_id_type=pl.DeviceIdType.MESH)

    def launch(key, src, dst, way):
        copy = copy_of(key, src, dst, way)
        copy.start()
        started.append(copy)

    def arrive(key, dst, way="x"):
        copy_of(key, dst, dst, way).wait_recv()

    def block(kind, dz, px, py, half=None):
        zz, yy = wrap(z + dz), lax.rem(y + py, NY)
        xx = lax.rem(x + px, NX)
        if kind == "U":
            size = depth if half is None else depth // 2
            at = fs_of(zz, yy, xx) * depth + (0 if half in (None, 0) else size)
            return u_buf.at[pl.ds(pl.multiple_of(at, size), size), :]
        size = wide if half is None else wide // 2
        at = 0 if half in (None, 0) else size
        return d_buf.at[zz * NY + yy, pl.ds(at, size), pl.ds(pl.multiple_of(xx * cols, cols), cols)]

    def column(kind, *ways):
        for k in ways:
            src, dst = (half_of(k)[0], own_up) if kind == "U" else (half_of(k)[1], own_down)
            launch((kind, nz - k, 0, 0, None), src, dst, k)

    def take(kind, dz, px, py, half=None):
        arrive((kind, dz, px, py, half), block(kind, dz, px, py, half))

    def share(kind, dz):
        if dz:
            take(kind, dz, 0, 0)
        ref = block(kind, dz, 0, 0)
        launch((kind, dz, 1, 0, None), ref, ref, "x")
        launch((kind, dz, 0, 1, None), ref, ref, "y")

    def cross(kind, dz):
        for px, py, way, half in ((1, 0, "y", 0), (0, 1, "x", 1)):
            take(kind, dz, px, py)
            ref = block(kind, dz, px, py, half)
            launch((kind, dz, 1, 1, half), ref, ref, way)

    def corner(kind, dz):
        take(kind, dz, 1, 1, 0)
        take(kind, dz, 1, 1, 1)

    part_rows = rows // 2
    mine_rows = pl.ds(pl.multiple_of(c * part_rows, part_rows), part_rows)
    other_rows = pl.ds(pl.multiple_of((1 - c) * part_rows, part_rows), part_rows)
    column("U", 1, 3)
    local[0].wait()
    share("U", 0)
    cross("U", 0)
    share("U", 1)
    share("U", 3)
    column("U", 2)
    launch(("T", "x"), x_ref.at[mine_rows, :], t_buf.at[mine_rows, :], "peer")
    cross("U", 1)
    share("U", 2)
    column("D", 1, 3)
    cross("U", 3)
    local[1].wait()
    share("D", 0)
    cross("U", 2)
    arrive(("T", "x"), t_buf.at[mine_rows, :])
    launch(("T", "c"), t_buf.at[mine_rows, :], t_buf.at[mine_rows, :], "c")
    for dz in range(nz):
        corner("U", dz)

    tile_m, tile_n = 256, min(512, wide)

    def up_part(src, base):
        @pl.loop(0, wide // tile_n)
        def _(j):
            at = pl.ds(pl.multiple_of(j * tile_n, tile_n), tile_n)

            @pl.loop(0, rows // tile_m)
            def _(i):
                r = pl.multiple_of(i * tile_m, tile_m)
                pre = jnp.dot(src[pl.ds(r, tile_m), :], u_buf[:, at],
                              preferred_element_type=jnp.float32)
                act = jnp.square(jnp.maximum(pre * s_ref[:, at], 0.0))
                h_buf[pl.ds(base + r, tile_m), at] = act.astype(jnp.bfloat16)

    up_part(x_ref, 0)
    cross("D", 0)
    share("D", 1)
    share("D", 3)
    column("D", 2)
    arrive(("T", "c"), t_buf.at[other_rows, :])
    up_part(t_buf, rows)
    cross("D", 1)
    share("D", 2)
    cross("D", 3)

    stages = [((z + 1) % 2, 0), ((z + 1) % 2, 1), (z % 2, 0), (z % 2, 1)]

    def owned(n, core):
        q, dy = stages[n]
        return (q + core * (nz // 2)) * NY + lax.rem(y + dy, NY)

    def theirs(n):
        zy = owned(n, 1 - c)

        @pl.loop(0, 2 * rows // tile_m)
        def _(i):
            r = pl.ds(pl.multiple_of(i * tile_m, tile_m), tile_m)
            ssend[n, r, :] = jnp.dot(h_buf[r, :], d_buf[zy],
                                     preferred_element_type=jnp.float32).astype(jnp.bfloat16)

        launch(("S", n), ssend.at[n], srecv.at[n], "c")

    def mine(n):
        zy = owned(n, c)
        arrive(("S", n), srecv.at[n])

        def total(i):
            r = pl.ds(pl.multiple_of(i, tile_m), tile_m)
            return jnp.dot(h_buf[r, :], d_buf[zy],
                           preferred_element_type=jnp.float32) + srecv[n, r, :].astype(jnp.float32)

        @pl.loop(0, rows // tile_m)
        def _(i):
            r = pl.multiple_of(i * tile_m, tile_m)
            xsend[n, pl.ds(r, tile_m), :] = total(rows + r).astype(jnp.bfloat16)

        met = (n + 2) % 4
        launch(("X", met), xsend.at[n], xrecv.at[met], "peer")

        @pl.loop(0, rows // tile_m)
        def _(i):
            r = pl.multiple_of(i * tile_m, tile_m)
            keep[n, pl.ds(r, tile_m), :] = total(r)

    def finish(n):
        arrive(("X", n), xrecv.at[n])
        at = pl.multiple_of((owned(n, c) - c * (nz // 2) * NY) * pair, pair)
        out_ref[:, pl.ds(at, pair)] = (keep[n] + xrecv[n].astype(jnp.float32)).astype(out_ref.dtype)

    theirs(0)
    corner("D", 1)
    corner("D", 3)
    theirs(1)
    mine(0)
    cross("D", 2)
    theirs(2)
    mine(1)
    corner("D", 0)
    corner("D", 2)
    theirs(3)
    mine(2)
    mine(3)
    for n in (2, 3, 0, 1):
        finish(n)
    for copy in started:
        copy.wait_send()


def fused(nz, tokens, norm_gain, up_weight, up_scale, down_weight, down_scale):
    rows, width = tokens.shape
    depth, hidden = up_weight.shape
    cols = down_weight.shape[1]
    wide = hidden // 2
    side = lax.rem(lax.axis_index("fs") // (NX * NY), 2)
    own_scale = lax.dynamic_slice_in_dim(up_scale, side * wide, wide, 0)[None]
    ways = 2 * (nz - 1 + 4 * nz) + 2 + 8
    vmem = pl.BlockSpec(memory_space=pltpu.VMEM)
    return pl.pallas_call(
        functools.partial(kernel, nz),
        out_shape=jax.ShapeDtypeStruct((rows, width // 2), jnp.bfloat16),
        in_specs=[vmem] * 4,
        out_specs=vmem,
        scratch_shapes=[
            pltpu.VMEM((width, wide), jnp.bfloat16),
            pltpu.VMEM((nz * NY, wide, NX * cols), jnp.bfloat16),
            pltpu.VMEM((rows, width), jnp.bfloat16),
            pltpu.VMEM((2 * rows, wide), jnp.bfloat16),
            pltpu.VMEM((4, 2 * rows, NX * cols), jnp.bfloat16),
            pltpu.VMEM((4, 2 * rows, NX * cols), jnp.bfloat16),
            pltpu.VMEM((4, rows, NX * cols), jnp.bfloat16),
            pltpu.VMEM((4, rows, NX * cols), jnp.bfloat16),
            pltpu.VMEM((4, rows, NX * cols), jnp.float32),
            pltpu.SemaphoreType.DMA((ways,)),
            pltpu.SemaphoreType.DMA((ways,)),
            pltpu.SemaphoreType.DMA((2,)),
        ],
        compiler_params=pltpu.CompilerParams(
            collective_id=0, has_side_effects=True, vmem_limit_bytes=60 * 1024 * 1024
        ),
    )(
        normalise(tokens, norm_gain),
        own_scale,
        up_weight.astype(jnp.bfloat16),
        (down_weight * down_scale).astype(jnp.bfloat16),
    )


def solution(mesh):
    in_specs = (P("fs", None), P(), P("fs", "tp"), P("tp", "fs"), P("fs"))
    in_specs = in_specs[:3] + (P("tp"),) + in_specs[3:]
    out_specs = P("fs", "tp")
    nz = mesh.shape["fs"] // (NX * NY)
    local = functools.partial(fused, nz) if nz == 4 and mesh.shape["tp"] == 2 else plain
    return jax.shard_map(local, mesh=mesh, in_specs=in_specs, out_specs=out_specs, check_vma=False)
```

profile of v0, /device:TPU:1, one launch (start us, length us, event | category | flops | bytes accessed | tf_op | source)
XLA Modules:
  0.0 203.6 jit_solution(1550454538272228547)
XLA Ops:
  0.0 0.0 copy-start.4
  0.0 0.0 copy-start.1
  0.0 0.0 copy-start.2
  0.0 0.0 copy-start.5
  0.0 2.7 %fusion = f32[768]{0:T(1024)S(1)} fusion(bf16[768,2048]{1,0:T(8,128)(2,1)} %param.6), kind=kLoop, calls=%fused_computation.2 | loop fusion | flops 4717824 | bytes 3148800 | tf_op jit(solution)/shard_map/reduce_sum | solution.py:15
  2.8 0.0 copy-done.4
  2.8 0.6 dynamic_slice.3
  3.4 0.0 copy-done.1
  3.4 0.0 copy-start
  3.4 0.0 copy-start.3
  3.4 1.1 convert_element_type.14.up_ref
  4.5 0.0 copy-done.2
  4.5 0.0 copy-done.5
  4.5 1.1 multiply_convert_fusion.down_ref
  5.6 0.2 copy-done
  5.9 0.0 copy-done.3
  5.9 2.4 %fusion.2.x_ref = bf16[768,2048]{1,0:T(8,128)(2,1)} fusion(bf16[768,2048]{1,0:T(8,128)(2,1)S(1)} %copy-done, f32[2048]{0:T(1024)S(1)} %copy-done.3, f32[768]{0:T(1024)S(1)} %add_rsqrt_fusion), kind=kLoop, calls=%fused_computation.4 | loop fusion | flops 6291456 | bytes 6302720 | tf_op jit(solution)/shard_map/convert_element_type | solution.py:16
  8.3 192.6 %shard_map.64 = bf16[768,1024]{1,0:T(8,128)(2,1)} custom-call(bf16[768,2048]{1,0:T(8,128)(2,1)} %fusion.2.x_ref, f32[1,2048]{1,0:T(1,128)} %bitcast.1, bf16[128,4096]{1,0:T(8,128)(2,1)} %convert_element_type.14.up_ref, bf16[4096,128]{1,0:T(8,128)(2,1)} %multiply_convert_fusion.down_ref), custom_call_target="tpu_custom_call" | custom-call | tf_op jit(solution)/shard_map/pallas_call | solution.py:256
  200.9 2.7 %copy.8 = bf16[768,1024]{1,0:T(8,128)(2,1)} copy(bf16[768,1024]{1,0:T(8,128)(2,1)} %shard_map.64) | data formatting | bytes 3145728
  (1 shorter events, 0.0 us)
Async XLA Ops:
  0.0 2.8 %copy-start.4 = (f32[4096]{0:T(1024)S(1)}, f32[4096]{0:T(1024)}, u32[]{:S(2)}) copy-start(f32[4096]{0:T(1024)} %param.9) | copy-start | bytes 49156
  0.0 3.4 %copy-start.1 = (f32[128,4096]{1,0:T(8,128)S(1)}, f32[128,4096]{1,0:T(8,128)}, u32[]{:S(2)}) copy-start(f32[128,4096]{1,0:T(8,128)} %param.8) | copy-start | bytes 6291460
  0.0 4.5 %copy-start.2 = (f32[4096,128]{1,0:T(8,128)S(1)}, f32[4096,128]{1,0:T(8,128)}, u32[]{:S(2)}) copy-start(f32[4096,128]{1,0:T(8,128)} %param.10) | copy-start | bytes 6291460
  0.0 4.5 %copy-start.5 = (f32[128]{0:T(128)S(1)}, f32[128]{0:T(128)}, u32[]{:S(2)}) copy-start(f32[128]{0:T(128)} %param.11) | copy-start | bytes 1540
  3.4 2.5 %copy-start = (bf16[768,2048]{1,0:T(8,128)(2,1)S(1)}, bf16[768,2048]{1,0:T(8,128)(2,1)}, u32[]{:S(2)}) copy-start(bf16[768,2048]{1,0:T(8,128)(2,1)} %param.6) | copy-start | bytes 9437188
  3.4 2.5 %copy-start.3 = (f32[2048]{0:T(1024)S(1)}, f32[2048]{0:T(1024)}, u32[]{:S(2)}) copy-start(f32[2048]{0:T(1024)} %param.7) | copy-start | bytes 24580
where the time goes:
time: 206 us; the launch traced here: 204 us
  Pallas kernels  193 us (94%)
  other arithmetic  7.41 us (4%)
  local copies, waits for them, and re-layouts  3.52 us (2%)
    pallas_call x1, Pallas kernels, fused(): pl.pallas_call(functools.partial(kernel, nz), out_shape=jax.ShapeDtypeStr...  193 us

commit v1 on v0

v1 whole, which is shorter than its diff:
```python
import jax
import jax.numpy as jnp
from jax import lax
from jax.experimental import pallas as pl
from jax.experimental.pallas import tpu as pltpu
from jax.sharding import PartitionSpec as P

epsilon = 1e-06


def normalise(tokens, norm_gain):
    floats = tokens.astype(jnp.float32)
    inverse = lax.rsqrt(jnp.mean(floats * floats, axis=-1, keepdims=True) + epsilon)
    return (floats * inverse * norm_gain).astype(jnp.bfloat16)


def plain(tokens, norm_gain, up_weight, up_scale, down_weight, down_scale):
    normed = normalise(tokens, norm_gain)
    up_whole = lax.all_gather(up_weight.astype(jnp.bfloat16), "fs", axis=0, tiled=True)
    up_pre = jnp.dot(normed, up_whole, preferred_element_type=jnp.float32)
    scaled = (down_weight * down_scale).astype(jnp.bfloat16)
    down_whole = lax.all_gather(scaled, "fs", axis=1, tiled=True)
    hidden = jnp.square(jax.nn.relu(up_pre * up_scale)).astype(jnp.bfloat16)
    partial_value = jnp.dot(hidden, down_whole, preferred_element_type=jnp.float32)
    return lax.psum_scatter(
        partial_value.astype(jnp.bfloat16), "tp", scatter_dimension=1, tiled=True
    )


NX, NY = 2, 2
order = (0, 1, 3, 2)


def kernel(tok_ref, gain_ref, s_ref, up_ref, down_ref, dscale_ref, out_ref,
           x_buf, u_in, d_in, u_send, d_send, u_buf, d_buf, t_buf, h_buf, ssend, srecv,
           xsend, xrecv, keep, part, send_sems, recv_sems, local_sems):
    me = lax.axis_index("fs")
    c = lax.axis_index("tp")
    x = lax.rem(me, NX)
    y = lax.rem(me // NX, NY)
    z = me // (NX * NY)
    side = lax.rem(z, 2)
    rows = x_buf.shape[0]
    depth = u_send.shape[0]
    wide = u_send.shape[1]
    cols = d_send.shape[1]
    pair = NX * cols
    part_rows = rows // 2

    def fs_of(zz, yy, xx):
        return (zz * NY + yy) * NX + xx

    def level(k):
        return {0: z, 1: z + 1 - 2 * side, 2: lax.rem(z + 2, 4), 3: 3 - z}[k]

    target = {
        **{k: {"fs": fs_of(level(k), y, x), "tp": c} for k in (1, 2, 3)},
        "y": {"fs": fs_of(z, 1 - y, x), "tp": c},
        "x": {"fs": fs_of(z, y, 1 - x), "tp": c},
        "c": {"fs": me, "tp": 1 - c},
    }
    peer = 1

    mine_rows = pl.ds(pl.multiple_of(c * part_rows, part_rows), part_rows)
    other_rows = pl.ds(pl.multiple_of((1 - c) * part_rows, part_rows), part_rows)
    local = [
        pltpu.make_async_copy(up_ref, u_in, local_sems.at[0]),
        pltpu.make_async_copy(tok_ref, x_buf, local_sems.at[1]),
        pltpu.make_async_copy(down_ref, d_in, local_sems.at[2]),
    ]
    for copy in local:
        copy.start()

    barrier = pltpu.get_barrier_semaphore()
    for where in target.values():
        pl.semaphore_signal(barrier, inc=1, device_id=where, device_id_type=pl.DeviceIdType.MESH)

    slots, started = {}, []

    def copy_of(key, src, dst, way):
        n = slots.setdefault(key, len(slots))
        return pltpu.make_async_remote_copy(
            src_ref=src, dst_ref=dst, send_sem=send_sems.at[n], recv_sem=recv_sems.at[n],
            device_id=target[way], device_id_type=pl.DeviceIdType.MESH)

    def launch(key, src, dst, way):
        copy = copy_of(key, src, dst, way)
        copy.start()
        started.append(copy)

    def arrive(key, dst, way="x"):
        copy_of(key, dst, dst, way).wait_recv()

    def block(kind, k, px, py, half=None):
        zz, yy = level(k), lax.rem(y + py, NY)
        xx = lax.rem(x + px, NX)
        if kind == "U":
            size = depth if half is None else depth // 2
            at = fs_of(zz, yy, xx) * depth + (0 if half in (None, 0) else size)
            return u_buf.at[pl.ds(pl.multiple_of(at, size), size), :]
        size = wide if half is None else wide // 2
        at = 0 if half in (None, 0) else size
        return d_buf.at[zz * NY + yy, pl.ds(at, size), pl.ds(pl.multiple_of(xx * cols, cols), cols)]

    own = {kind: block(kind, 0, 0, 0) for kind in "UD"}
    other = {"U": u_send, "D": d_send}

    def column(kind, k):
        launch((kind, k, 0, 0, None), own[kind] if k == 2 else other[kind], own[kind], k)

    def take(kind, k, px, py, half=None):
        arrive((kind, k, px, py, half), block(kind, k, px, py, half))

    def share(kind, k):
        if k:
            take(kind, k, 0, 0)
        ref = block(kind, k, 0, 0)
        launch((kind, k, 1, 0, None), ref, ref, "x")
        launch((kind, k, 0, 1, None), ref, ref, "y")

    def cross(kind, k):
        for px, py, way, half in ((1, 0, "y", 0), (0, 1, "x", 1)):
            take(kind, k, px, py)
            ref = block(kind, k, px, py, half)
            launch((kind, k, 1, 1, half), ref, ref, way)

    def corner(kind, k):
        take(kind, k, 1, 1, 0)
        take(kind, k, 1, 1, 1)

    at_own = pl.ds(pl.multiple_of(side * wide, wide), wide)
    at_other = pl.ds(pl.multiple_of((1 - side) * wide, wide), wide)

    local[0].wait()
    u_send[...] = u_in[:, at_other].astype(jnp.bfloat16)
    own["U"][...] = u_in[:, at_own].astype(jnp.bfloat16)
    pl.semaphore_wait(barrier, len(target))
    column("U", 1)
    share("U", 0)
    column("U", 3)
    column("U", 2)

    local[2].wait()
    d_send[...] = (d_in[at_other, :] * dscale_ref[...]).astype(jnp.bfloat16)
    own["D"][...] = (d_in[at_own, :] * dscale_ref[...]).astype(jnp.bfloat16)

    step = 16

    def normalise_rows(base):
        @pl.loop(0, part_rows // step)
        def _(i):
            r = pl.ds(pl.multiple_of(base + i * step, step), step)
            floats = x_buf[r, :].astype(jnp.float32)
            inverse = lax.rsqrt(jnp.mean(floats * floats, axis=-1, keepdims=True) + epsilon)
            x_buf[r, :] = (floats * inverse * gain_ref[...]).astype(jnp.bfloat16)

    local[1].wait()
    normalise_rows(c * part_rows)
    column("D", 1)
    column("D", 3)
    launch(("T", "x"), x_buf.at[mine_rows, :], t_buf.at[mine_rows, :], peer)
    column("D", 2)
    normalise_rows((1 - c) * part_rows)

    share("U", 1)
    cross("U", 0)
    cross("U", 1)
    share("U", 3)
    share("U", 2)
    cross("U", 3)
    cross("U", 2)
    share("D", 0)
    share("D", 1)
    for k in order:
        corner("U", k)

    tile_m, tile_n = part_rows, min(512, wide)
    chunks = wide // tile_n

    def up_part(src, base, first, count, jfirst=0, jcount=chunks):
        @pl.loop(jfirst, jfirst + jcount)
        def _(j):
            at = pl.ds(pl.multiple_of(j * tile_n, tile_n), tile_n)
            at_s = pl.ds(pl.multiple_of(side * wide + j * tile_n, tile_n), tile_n)

            for i in range(count):
                r = pl.multiple_of(first + i * tile_m, tile_m)
                pre = jnp.dot(src[pl.ds(r, tile_m), :], u_buf[:, at],
                              preferred_element_type=jnp.float32)
                act = jnp.square(jnp.maximum(pre * s_ref[:, at_s], 0.0))
                h_buf[pl.ds(base + r, tile_m), at] = act.astype(jnp.bfloat16)

    up_part(x_buf, 0, 0, 2)
    cross("D", 0)
    arrive(("T", "x"), t_buf.at[mine_rows, :])
    launch(("T", "c"), t_buf.at[mine_rows, :], t_buf.at[mine_rows, :], "c")
    cross("D", 1)
    up_part(t_buf, rows, c * part_rows, 1)
    share("D", 3)
    arrive(("T", "c"), t_buf.at[other_rows, :])
    up_part(t_buf, rows, (1 - c) * part_rows, 1)

    span = rows // 2

    def dots(base, zy, put):
        @pl.loop(0, rows // span)
        def _(i):
            r = pl.multiple_of(i * span, span)
            put(pl.ds(r, span), jnp.dot(h_buf[pl.ds(base + r, span), :], d_buf[zy],
                                        preferred_element_type=jnp.float32))

    finals = []

    def stage(k, py):
        j = order.index(k)
        zz, yy = level(k), lax.rem(y + py, NY)
        zy = zz * NY + yy
        n = (j % 2) * 2 + py
        met = (n + 2) % 4
        mine = zz // 2 == c

        @pl.when(jnp.logical_not(mine))
        def _():
            for half, base in ((0, rows), (1, 0)):
                ref = ssend.at[n, half]

                def put(r, value):
                    ssend[n, half, r, :] = value.astype(jnp.bfloat16)

                dots(base, zy, put)
                copy_of(("S", n, half), ref, srecv.at[n, half], "c").start()

        @pl.when(mine)
        def _():
            def put(r, value):
                part[r, :] = value

            dots(rows, zy, put)
            arrive(("S", n, 0), srecv.at[n, 0])
            xsend[n] = (part[...] + srecv[n, 0].astype(jnp.float32)).astype(jnp.bfloat16)
            copy_of(("X", met), xsend.at[n], xrecv.at[met], peer).start()

            def put_keep(r, value):
                keep[n, r, :] = value

            dots(0, zy, put_keep)
            arrive(("S", n, 1), srecv.at[n, 1])
            keep[n] = keep[n] + srecv[n, 1].astype(jnp.float32)

    def finish(k, py):
        j = order.index(k)
        zz, yy = level(k), lax.rem(y + py, NY)
        n = (j % 2) * 2 + py
        met = (n + 2) % 4

        @pl.when(zz // 2 == c)
        def _():
            arrive(("X", n), xrecv.at[n])
            at = pl.multiple_of((lax.rem(zz, 2) * NY + yy) * pair, pair)
            out_ref[:, pl.ds(at, pair)] = (keep[n] + xrecv[n].astype(jnp.float32)).astype(out_ref.dtype)
            copy_of(("X", met), xsend.at[n], xrecv.at[met], peer).wait_send()

        @pl.when(zz // 2 != c)
        def _():
            for half in range(2):
                copy_of(("S", n, half), ssend.at[n, half], srecv.at[n, half], "c").wait_send()

    stage(0, 0)
    corner("D", 0)
    stage(0, 1)
    share("D", 2)
    stage(1, 0)
    corner("D", 1)
    stage(1, 1)
    cross("D", 3)
    stage(3, 0)
    cross("D", 2)
    stage(2, 0)
    for py in range(2):
        finish(0, py)
        finish(1, py)
    corner("D", 3)
    stage(3, 1)
    corner("D", 2)
    stage(2, 1)
    for k, py in ((3, 0), (2, 0), (3, 1), (2, 1)):
        finish(k, py)
    for copy in started:
        copy.wait_send()


def fused(tokens, norm_gain, up_weight, up_scale, down_weight, down_scale):
    rows, width = tokens.shape
    depth, hidden = up_weight.shape
    cols = down_weight.shape[1]
    wide = hidden // 2
    nz = 4
    pair = NX * cols
    ways = 2 * (nz - 1 + 4 * nz) + 2 + 12
    vmem = pl.BlockSpec(memory_space=pltpu.VMEM)
    hbm = pl.BlockSpec(memory_space=pl.ANY)
    return pl.pallas_call(
        kernel,
        out_shape=jax.ShapeDtypeStruct((rows, width // 2), jnp.bfloat16),
        in_specs=[hbm, vmem, vmem, hbm, hbm, vmem],
        out_specs=vmem,
        scratch_shapes=[
            pltpu.VMEM((rows, width), jnp.bfloat16),
            pltpu.VMEM((depth, hidden), jnp.float32),
            pltpu.VMEM((hidden, cols), jnp.float32),
            pltpu.VMEM((depth, wide), jnp.bfloat16),
            pltpu.VMEM((wide, cols), jnp.bfloat16),
            pltpu.VMEM((width, wide), jnp.bfloat16),
            pltpu.VMEM((nz * NY, wide, pair), jnp.bfloat16),
            pltpu.VMEM((rows, width), jnp.bfloat16),
            pltpu.VMEM((2 * rows, wide), jnp.bfloat16),
            pltpu.VMEM((4, 2, rows, pair), jnp.bfloat16),
            pltpu.VMEM((4, 2, rows, pair), jnp.bfloat16),
            pltpu.VMEM((4, rows, pair), jnp.bfloat16),
            pltpu.VMEM((4, rows, pair), jnp.bfloat16),
            pltpu.VMEM((4, rows, pair), jnp.float32),
            pltpu.VMEM((rows, pair), jnp.float32),
            pltpu.SemaphoreType.DMA((ways,)),
            pltpu.SemaphoreType.DMA((ways,)),
            pltpu.SemaphoreType.DMA((3,)),
        ],
        compiler_params=pltpu.CompilerParams(
            collective_id=0, has_side_effects=True, vmem_limit_bytes=60 * 1024 * 1024
        ),
    )(tokens, norm_gain[None], up_scale[None], up_weight, down_weight, down_scale[None])


def solution(mesh):
    in_specs = (P("fs", None), P(), P("fs", "tp"), P("tp"), P("tp", "fs"), P("fs"))
    out_specs = P("fs", "tp")
    nz = mesh.shape["fs"] // (NX * NY)
    local = fused if nz == 4 and mesh.shape["tp"] == 2 else plain
    return jax.shard_map(local, mesh=mesh, in_specs=in_specs, out_specs=out_specs, check_vma=False)
```

time: 206 us -> 161 us (0.78); the launches traced: 204 us -> 161 us
  Pallas kernels: 193 us -> 158 us
  other arithmetic: 7.41 us -> 0 us
    pallas_call x1, Pallas kernels: 193 us -> 158 us  [fused(): pl.pallas_call(kernel, out_shape=jax.ShapeDtypeStruct((rows, width // 2),...]
    convert_element_type x3 -> x0, other arithmetic: 4.68 us -> none  [the longest x1 2.43 us: normalise(): return (floats * inverse * norm_gain).astype(jnp.bfloat16)]
    reduce_sum x1 -> x0, other arithmetic: 2.72 us -> none  [normalise(): jnp.mean(floats * floats, axis=-1, keepdims=True) + epsilon]
where the time goes in v1:
time: 161 us
  Pallas kernels  158 us (98%)
  local copies, waits for them, and re-layouts  2.67 us (2%)
    pallas_call x1, Pallas kernels, fused(): pl.pallas_call(kernel, out_shape=jax.ShapeDtypeStruct((rows, width // 2),...  158 us

profile of v1, /device:TPU:1, one launch (start us, length us, event | category | flops | bytes accessed | tf_op | source)
XLA Modules:
  0.0 160.8 jit_solution(11115949113213590148)
XLA Ops:
  0.0 158.1 %shard_map.64 = bf16[768,1024]{1,0:T(8,128)(2,1)} custom-call(bf16[768,2048]{1,0:T(8,128)(2,1)} %tok_ref.1, f32[1,2048]{1,0:T(1,128)} %bitcast.4, f32[1,4096]{1,0:T(1,128)} %bitcast.3, f32[128,4096]{1,0:T(8,128)} %up_ref.1, f32[4096,128]{1,0:T(8,128)} %down_ref.1, f32[1,128]{1,0:T(1,128)} %bitcast.5), custom_call_target="tpu_custom_call" | custom-call | tf_op jit(solution)/shard_map/pallas_call | solution.py:302
  158.2 2.7 %copy.8 = bf16[768,1024]{1,0:T(8,128)(2,1)} copy(bf16[768,1024]{1,0:T(8,128)(2,1)} %shard_map.64) | data formatting | bytes 3145728

commit v2 on v1

--- a/solution.py
+++ b/solution.py
@@ -31,8 +31,8 @@
 order = (0, 1, 3, 2)
 
 
-def kernel(tok_ref, gain_ref, s_ref, up_ref, down_ref, dscale_ref, out_ref,
-           x_buf, u_in, d_in, u_send, d_send, u_buf, d_buf, t_buf, h_buf, ssend, srecv,
+def kernel(tok_ref, gain_hbm, s_hbm, up_ref, down_ref, dscale_hbm, out_ref,
+           gain_ref, s_ref, dscale_ref, x_buf, u_in, d_in, u_send, d_send, u_buf, d_buf, t_buf, h_buf, ssend, srecv,
            xsend, xrecv, keep, part, send_sems, recv_sems, local_sems):
     me = lax.axis_index("fs")
     c = lax.axis_index("tp")
@@ -63,10 +63,16 @@
 
     mine_rows = pl.ds(pl.multiple_of(c * part_rows, part_rows), part_rows)
     other_rows = pl.ds(pl.multiple_of((1 - c) * part_rows, part_rows), part_rows)
+    at_own = pl.ds(pl.multiple_of(side * wide, wide), wide)
+    at_other = pl.ds(pl.multiple_of((1 - side) * wide, wide), wide)
     local = [
-        pltpu.make_async_copy(up_ref, u_in, local_sems.at[0]),
+        pltpu.make_async_copy(up_ref.at[:, at_own], u_in.at[:, at_own], local_sems.at[0]),
+        pltpu.make_async_copy(up_ref.at[:, at_other], u_in.at[:, at_other], local_sems.at[3]),
         pltpu.make_async_copy(tok_ref, x_buf, local_sems.at[1]),
         pltpu.make_async_copy(down_ref, d_in, local_sems.at[2]),
+        pltpu.make_async_copy(gain_hbm, gain_ref, local_sems.at[4]),
+        pltpu.make_async_copy(s_hbm, s_ref, local_sems.at[5]),
+        pltpu.make_async_copy(dscale_hbm, dscale_ref, local_sems.at[6]),
     ]
     for copy in local:
         copy.start()
@@ -75,12 +81,13 @@
     for where in target.values():
         pl.semaphore_signal(barrier, inc=1, device_id=where, device_id_type=pl.DeviceIdType.MESH)
 
-    slots, started = {}, []
-
-    def copy_of(key, src, dst, way):
+    slots, started, guarded = {}, [], []
+
+    def copy_of(key, src, dst, way, sent=None):
         n = slots.setdefault(key, len(slots))
+        m = n if sent is None else slots.setdefault(sent, len(slots))
         return pltpu.make_async_remote_copy(
-            src_ref=src, dst_ref=dst, send_sem=send_sems.at[n], recv_sem=recv_sems.at[n],
+            src_ref=src, dst_ref=dst, send_sem=send_sems.at[m], recv_sem=recv_sems.at[n],
             device_id=target[way], device_id_type=pl.DeviceIdType.MESH)
 
     def launch(key, src, dst, way):
@@ -105,14 +112,34 @@
     own = {kind: block(kind, 0, 0, 0) for kind in "UD"}
     other = {"U": u_send, "D": d_send}
 
-    def column(kind, k):
-        launch((kind, k, 0, 0, None), own[kind] if k == 2 else other[kind], own[kind], k)
+    inner = (z + 1) // 2 == 1
+    outer = jnp.logical_not(inner)
+
+    def launch_if(where, copy):
+        @pl.when(where)
+        def _():
+            copy.start()
+
+        guarded.append((where, copy))
+
+    def column(kind, k, where=None):
+        copy = copy_of((kind, k, 0, 0, None), own[kind] if k == 2 else other[kind], own[kind], k)
+        if where is None:
+            copy.start()
+            started.append(copy)
+        else:
+            launch_if(where, copy)
+
+    def relay(kind):
+        take(kind, 1, 0, 0)
+        ref = block(kind, 1, 0, 0)
+        launch_if(inner, copy_of((kind, 3, 0, 0, None), ref, ref, 2, ("R", kind)))
 
     def take(kind, k, px, py, half=None):
         arrive((kind, k, px, py, half), block(kind, k, px, py, half))
 
     def share(kind, k):
-        if k:
+        if k > 1:
             take(kind, k, 0, 0)
         ref = block(kind, k, 0, 0)
         launch((kind, k, 1, 0, None), ref, ref, "x")
@@ -128,19 +155,18 @@
         take(kind, k, 1, 1, 0)
         take(kind, k, 1, 1, 1)
 
-    at_own = pl.ds(pl.multiple_of(side * wide, wide), wide)
-    at_other = pl.ds(pl.multiple_of((1 - side) * wide, wide), wide)
-
     local[0].wait()
+    own["U"][...] = u_in[:, at_own].astype(jnp.bfloat16)
+    local[1].wait()
     u_send[...] = u_in[:, at_other].astype(jnp.bfloat16)
-    own["U"][...] = u_in[:, at_own].astype(jnp.bfloat16)
     pl.semaphore_wait(barrier, len(target))
     column("U", 1)
     share("U", 0)
-    column("U", 3)
-    column("U", 2)
-
-    local[2].wait()
+    column("U", 3, inner)
+    column("U", 2, outer)
+
+    for copy in local[3:]:
+        copy.wait()
     d_send[...] = (d_in[at_other, :] * dscale_ref[...]).astype(jnp.bfloat16)
     own["D"][...] = (d_in[at_own, :] * dscale_ref[...]).astype(jnp.bfloat16)
 
@@ -154,22 +180,26 @@
             inverse = lax.rsqrt(jnp.mean(floats * floats, axis=-1, keepdims=True) + epsilon)
             x_buf[r, :] = (floats * inverse * gain_ref[...]).astype(jnp.bfloat16)
 
-    local[1].wait()
+    local[2].wait()
     normalise_rows(c * part_rows)
     column("D", 1)
-    column("D", 3)
     launch(("T", "x"), x_buf.at[mine_rows, :], t_buf.at[mine_rows, :], peer)
-    column("D", 2)
     normalise_rows((1 - c) * part_rows)
 
+    relay("U")
     share("U", 1)
+    column("U", 2, inner)
     cross("U", 0)
     cross("U", 1)
+    share("D", 0)
     share("U", 3)
     share("U", 2)
     cross("U", 3)
+    relay("D")
+    column("D", 3, inner)
+    column("D", 2)
     cross("U", 2)
-    share("D", 0)
+    cross("D", 0)
     share("D", 1)
     for k in order:
         corner("U", k)
@@ -191,25 +221,15 @@
                 h_buf[pl.ds(base + r, tile_m), at] = act.astype(jnp.bfloat16)
 
     up_part(x_buf, 0, 0, 2)
-    cross("D", 0)
+    share("D", 3)
     arrive(("T", "x"), t_buf.at[mine_rows, :])
     launch(("T", "c"), t_buf.at[mine_rows, :], t_buf.at[mine_rows, :], "c")
-    cross("D", 1)
     up_part(t_buf, rows, c * part_rows, 1)
-    share("D", 3)
     arrive(("T", "c"), t_buf.at[other_rows, :])
     up_part(t_buf, rows, (1 - c) * part_rows, 1)
-
-    span = rows // 2
-
-    def dots(base, zy, put):
-        @pl.loop(0, rows // span)
-        def _(i):
-            r = pl.multiple_of(i * span, span)
-            put(pl.ds(r, span), jnp.dot(h_buf[pl.ds(base + r, span), :], d_buf[zy],
-                                        preferred_element_type=jnp.float32))
-
-    finals = []
+    cross("D", 1)
+
+    pending = []
 
     def stage(k, py):
         j = order.index(k)
@@ -219,74 +239,81 @@
         met = (n + 2) % 4
         mine = zz // 2 == c
 
-        @pl.when(jnp.logical_not(mine))
-        def _():
-            for half, base in ((0, rows), (1, 0)):
-                ref = ssend.at[n, half]
-
-                def put(r, value):
-                    ssend[n, half, r, :] = value.astype(jnp.bfloat16)
-
-                dots(base, zy, put)
-                copy_of(("S", n, half), ref, srecv.at[n, half], "c").start()
+        def sum_of(half):
+            return copy_of(("S", n, half), ssend.at[n, half], srecv.at[n, half], "c")
+
+        def cross_of():
+            return copy_of(("X", met), xsend.at[n], xrecv.at[met], peer)
+
+        def land_of():
+            return copy_of(("X", n), xsend.at[n], xrecv.at[n], peer)
+
+        for half, base in ((0, rows), (1, 0)):
+            part[half] = jnp.dot(h_buf[pl.ds(base, rows), :], d_buf[zy],
+                                 preferred_element_type=jnp.float32)
+
+            @pl.when(jnp.logical_not(mine))
+            def _():
+                ssend[n, half] = part[half].astype(jnp.bfloat16)
+                sum_of(half).start()
 
         @pl.when(mine)
         def _():
-            def put(r, value):
-                part[r, :] = value
-
-            dots(rows, zy, put)
-            arrive(("S", n, 0), srecv.at[n, 0])
-            xsend[n] = (part[...] + srecv[n, 0].astype(jnp.float32)).astype(jnp.bfloat16)
-            copy_of(("X", met), xsend.at[n], xrecv.at[met], peer).start()
-
-            def put_keep(r, value):
-                keep[n, r, :] = value
-
-            dots(0, zy, put_keep)
-            arrive(("S", n, 1), srecv.at[n, 1])
-            keep[n] = keep[n] + srecv[n, 1].astype(jnp.float32)
-
-    def finish(k, py):
-        j = order.index(k)
-        zz, yy = level(k), lax.rem(y + py, NY)
-        n = (j % 2) * 2 + py
-        met = (n + 2) % 4
-
-        @pl.when(zz // 2 == c)
-        def _():
-            arrive(("X", n), xrecv.at[n])
-            at = pl.multiple_of((lax.rem(zz, 2) * NY + yy) * pair, pair)
-            out_ref[:, pl.ds(at, pair)] = (keep[n] + xrecv[n].astype(jnp.float32)).astype(out_ref.dtype)
-            copy_of(("X", met), xsend.at[n], xrecv.at[met], peer).wait_send()
-
-        @pl.when(zz // 2 != c)
-        def _():
-            for half in range(2):
-                copy_of(("S", n, half), ssend.at[n, half], srecv.at[n, half], "c").wait_send()
+            sum_of(0).wait_recv()
+            xsend[n] = (part[0] + srecv[n, 0].astype(jnp.float32)).astype(jnp.bfloat16)
+            cross_of().start()
+            sum_of(1).wait_recv()
+            keep[n] = part[1] + srecv[n, 1].astype(jnp.float32)
+
+        def finish():
+            @pl.when(mine)
+            def _():
+                at = pl.multiple_of((lax.rem(zz, 2) * NY + yy) * pair, pair)
+                land_of().wait_recv()
+                out_ref[:, pl.ds(at, pair)] = (keep[n] + xrecv[n].astype(jnp.float32)
+                                               ).astype(out_ref.dtype)
+
+        def drain():
+            @pl.when(mine)
+            def _():
+                cross_of().wait_send()
+
+            @pl.when(jnp.logical_not(mine))
+            def _():
+                for half in range(2):
+                    sum_of(half).wait_send()
+
+        pending.append((finish, drain))
 
     stage(0, 0)
+    share("D", 2)
     corner("D", 0)
     stage(0, 1)
-    share("D", 2)
     stage(1, 0)
+    cross("D", 3)
     corner("D", 1)
     stage(1, 1)
-    cross("D", 3)
     stage(3, 0)
     cross("D", 2)
     stage(2, 0)
-    for py in range(2):
-        finish(0, py)
-        finish(1, py)
     corner("D", 3)
     stage(3, 1)
+    for finish, _ in pending[:4]:
+        finish()
     corner("D", 2)
     stage(2, 1)
-    for k, py in ((3, 0), (2, 0), (3, 1), (2, 1)):
-        finish(k, py)
+    for finish, _ in pending[4:6]:
+        finish()
+    pending[7][0]()
+    pending[6][0]()
+    for _, drain in pending:
+        drain()
     for copy in started:
         copy.wait_send()
+    for where, copy in guarded:
+        @pl.when(where)
+        def _(copy=copy):
+            copy.wait_send()
 
 
 def fused(tokens, norm_gain, up_weight, up_scale, down_weight, down_scale):
@@ -296,15 +323,18 @@
     wide = hidden // 2
     nz = 4
     pair = NX * cols
-    ways = 2 * (nz - 1 + 4 * nz) + 2 + 12
+    ways = 2 * (2 * (nz - 1) + 6 * nz) + 2 + 40
     vmem = pl.BlockSpec(memory_space=pltpu.VMEM)
-    hbm = pl.BlockSpec(memory_space=pl.ANY)
+    hbm = pl.BlockSpec(memory_space=pltpu.HBM)
     return pl.pallas_call(
         kernel,
         out_shape=jax.ShapeDtypeStruct((rows, width // 2), jnp.bfloat16),
-        in_specs=[hbm, vmem, vmem, hbm, hbm, vmem],
+        in_specs=[hbm] * 6,
         out_specs=vmem,
         scratch_shapes=[
+            pltpu.VMEM((1, width), jnp.float32),
+            pltpu.VMEM((1, hidden), jnp.float32),
+            pltpu.VMEM((1, cols), jnp.float32),
             pltpu.VMEM((rows, width), jnp.bfloat16),
             pltpu.VMEM((depth, hidden), jnp.float32),
             pltpu.VMEM((hidden, cols), jnp.float32),
@@ -319,13 +349,13 @@
             pltpu.VMEM((4, rows, pair), jnp.bfloat16),
             pltpu.VMEM((4, rows, pair), jnp.bfloat16),
             pltpu.VMEM((4, rows, pair), jnp.float32),
-            pltpu.VMEM((rows, pair), jnp.float32),
+            pltpu.VMEM((2, rows, pair), jnp.float32),
             pltpu.SemaphoreType.DMA((ways,)),
             pltpu.SemaphoreType.DMA((ways,)),
-            pltpu.SemaphoreType.DMA((3,)),
+            pltpu.SemaphoreType.DMA((7,)),
         ],
         compiler_params=pltpu.CompilerParams(
-            collective_id=0, has_side_effects=True, vmem_limit_bytes=60 * 1024 * 1024
+            collective_id=0, has_side_effects=True, vmem_limit_bytes=52 * 1024 * 1024
         ),
     )(tokens, norm_gain[None], up_scale[None], up_weight, down_weight, down_scale[None])
 

time: 161 us -> 159 us (0.988)
  Pallas kernels: 158 us -> 156 us
    pallas_call x1, Pallas kernels: 158 us -> 156 us  [fused(): pl.pallas_call(kernel, out_shape=jax.ShapeDtypeStruct((rows, width // 2),...]
where the time goes in v2:
time: 159 us
  Pallas kernels  156 us (98%)
  local copies, waits for them, and re-layouts  3.21 us (2%)
    pallas_call x1, Pallas kernels, fused(): pl.pallas_call(kernel, out_shape=jax.ShapeDtypeStruct((rows, width // 2),...  156 us
    unnamed x7, local copies, waits for them, and re-layouts  3.21 us

profile of v2, /device:TPU:1, one launch (start us, length us, event | category | flops | bytes accessed | tf_op | source)
XLA Modules:
  0.0 158.8 jit_solution(13335819277798049557)
XLA Ops:
  0.0 0.0 copy-start
  0.0 0.7 copy-done
  0.7 0.0 copy-start.1
  0.7 0.7 copy-done.1
  1.4 0.0 copy-start.2
  1.4 0.7 copy-done.2
  2.1 155.6 %shard_map.64 = bf16[768,1024]{1,0:T(8,128)(2,1)S(1)} custom-call(bf16[768,2048]{1,0:T(8,128)(2,1)} %tok_ref.1, f32[1,2048]{1,0:T(1,128)S(1)} %bitcast.4, f32[1,4096]{1,0:T(1,128)S(1)} %bitcast.3, f32[128,4096]{1,0:T(8,128)} %up_ref.1, f32[4096,128]{1,0:T(8,128)} %down_ref.1, f32[1,128]{1,0:T(1,128)S(1)} %bitcast.5), custom_call_target="tpu_custom_call" | custom-call | tf_op jit(solution)/shard_map/pallas_call | solution.py:329
  157.6 1.1 copy.8
Async XLA Ops:
  0.0 0.7 copy-start
  0.7 0.7 copy-start.1
  1.4 0.7 copy-start.2
